TPU v7x, 512 devices: a whole 4x4x16 slice. The times are simulated.
512 devices in a mesh: sp: 16 (over z), dp: 32 (over y, x, core).
Axes of the slice: x: 4, y: 4, z: 16, core: 2. Of those that a mesh axis runs over, the one named last changes fastest.
Arguments:
- query_latent: bfloat16 [32, 2048, 768], P('dp', 'sp'), may hold values from -6 to 6
- keyvalue_latent: bfloat16 [32, 2048, 512], P('dp', 'sp'), may hold values from -6 to 6
- rope_key: bfloat16 [32, 2048, 32], P('dp', 'sp'), may hold values from -150 to 150
- query_gain: float32 [768], replicated, may hold values from 0.1 to 1.9
- keyvalue_gain: float32 [512], replicated, may hold values from 0.1 to 1.9
- narrow_query: bfloat16 [768, 1536], P('dp'), may hold values from -0.21875 to 0.21875
- broad_query: bfloat16 [768, 2560], P('dp'), may hold values from -0.21875 to 0.21875
- narrow_key: bfloat16 [512, 1024], P('dp'), may hold values from -0.25 to 0.25
- narrow_value: bfloat16 [512, 1024], P('dp'), may hold values from -0.25 to 0.25
- broad_key: bfloat16 [512, 2048], P('dp'), may hold values from -0.25 to 0.25
- broad_value: bfloat16 [512, 1024], P('dp'), may hold values from -0.25 to 0.25
Outputs:
- narrow_mixed: bfloat16 [32, 2048, 1024], P('dp', 'sp')
- broad_mixed: bfloat16 [32, 2048, 1024], P('dp', 'sp')
All inputs are finite; a program needn't handle non-finite values.
Results may differ from a plain program's by a relative error of at most 0.014.
The roundings to bfloat16 on the way count: a program that leaves them out, or rounds other values in their place, can miss the bound.
Values may be sent and summed in bfloat16 or wider, within the bound.
A program may use at most 64 MiB of HBM per device.

v0:
```python
import jax
import jax.numpy as jnp
from jax import lax
from jax.sharding import PartitionSpec as P

PLAIN_NARROW = 64
PLAIN_BROAD = 128
ROTARY = 32
VALUE_SIZE = 64


EPSILON = 1e-06
ROTARY_BASE = 10000.0


def sent_together(arrays, axis, dim, along):
    widths = [a.shape[along] for a in arrays]
    both = jnp.concatenate(arrays, axis=along)
    whole = lax.all_gather(both, axis, axis=dim, tiled=True)
    return tuple(jnp.split(whole, [sum(widths[:k]) for k in range(1, len(widths))], axis=along))


def sent_together_2(arrays, axis, split_dim, concat_dim, along):
    widths = [a.shape[along] for a in arrays]
    both = jnp.concatenate(arrays, axis=along)
    whole = lax.all_to_all(both, axis, split_axis=split_dim, concat_axis=concat_dim, tiled=True)
    return tuple(jnp.split(whole, [sum(widths[:k]) for k in range(1, len(widths))], axis=along))


def normalize(latent, gain_row):
    values = latent.astype(jnp.float32)
    scaled = values * lax.rsqrt(jnp.mean(values * values, axis=-1, keepdims=True) + EPSILON)
    return (scaled * gain_row).astype(jnp.bfloat16)


def rotate(values, positions):
    halfway = ROTARY // 2
    frequency = ROTARY_BASE ** (-jnp.arange(halfway, dtype=jnp.float32) / halfway)
    angles = positions[:, None] * frequency[None, :]
    cosine = jnp.cos(angles)[:, None, :]
    sine_part = jnp.sin(angles)[:, None, :]
    width = values.shape[-1]
    plain_part = values[..., : width - ROTARY]
    first_half = values[..., width - ROTARY : width - halfway]
    second_half = values[..., width - halfway :]
    return jnp.concatenate(
        [
            plain_part,
            first_half * cosine - second_half * sine_part,
            first_half * sine_part + second_half * cosine,
        ],
        axis=-1,
    )


def make_fold(latent, pieces):
    return tuple(
        (jnp.dot(latent, weight_rows, preferred_element_type=jnp.float32) for weight_rows in pieces)
    )


def arrange(sums, width, positions, groups, with_rotary):
    row_count = positions.shape[0]
    shaped = sums.reshape(row_count, -1, width)
    if with_rotary:
        shaped = rotate(shaped, positions)
    shaped = shaped.astype(jnp.bfloat16)
    return shaped.reshape(row_count, groups, shaped.shape[1] // groups, width)


def attend_group(queries, keys_plain, values, rope_keys, factor):
    length = queries.shape[0]
    block_rows = 512
    key_whole = jnp.concatenate([keys_plain[:, 0, :], rope_keys], axis=1)
    value_head = values[:, 0, :]

    def one_block(query_block):
        scores = (
            jnp.einsum("qd,kd->qk", query_block, key_whole, preferred_element_type=jnp.float32)
            * factor
        )
        shifted = jnp.exp(scores - jnp.max(scores, axis=-1, keepdims=True))
        totals = jnp.sum(shifted, axis=-1, keepdims=True)
        mixed = jnp.dot(
            shifted.astype(jnp.bfloat16), value_head, preferred_element_type=jnp.float32
        )
        return (mixed / totals).astype(jnp.bfloat16)

    blocks = lax.map(one_block, queries[:, 0, :].reshape(length // block_rows, block_rows, -1))
    results = [blocks.reshape(length, -1)]
    return jnp.stack(results, axis=1)


def attend_both(members, rope_keys):
    query_first, key_first, value_first, query_second, key_second, value_second = members
    mixed_first = attend_group(
        query_first[:, 0],
        key_first[:, 0],
        value_first[:, 0],
        rope_keys,
        (PLAIN_NARROW + ROTARY) ** (-0.5),
    )
    mixed_second = attend_group(
        query_second[:, 0],
        key_second[:, 0],
        value_second[:, 0],
        rope_keys,
        (PLAIN_BROAD + ROTARY) ** (-0.5),
    )
    return (mixed_first[:, None], mixed_second[:, None])


def finish(mixed):
    flattened = mixed.reshape(mixed.shape[0], -1).astype(jnp.float32)
    scaled = flattened * lax.rsqrt(
        jnp.mean(flattened * flattened, axis=-1, keepdims=True) + EPSILON
    )
    return scaled.astype(jnp.bfloat16)[None]


def on_device(
    query_latent,
    keyvalue_latent,
    rope_key,
    query_gain,
    keyvalue_gain,
    narrow_query,
    broad_query,
    narrow_key,
    narrow_value,
    broad_key,
    broad_value,
):
    tokens = query_latent.shape[1]
    spread = lax.axis_size("sp")
    device_index = lax.axis_index("sp")
    width_narrow = PLAIN_NARROW + ROTARY
    width_broad = PLAIN_BROAD + ROTARY
    query_normed = normalize(query_latent[0], query_gain)
    pair_normed = normalize(keyvalue_latent[0], keyvalue_gain)
    own_positions = (device_index * tokens + jnp.arange(tokens, dtype=jnp.int32)).astype(
        jnp.float32
    )
    rope_own = rotate(rope_key[0].astype(jnp.float32)[:, None, :], own_positions)[:, 0, :].astype(
        jnp.bfloat16
    )
    query_all, pair_all, rope_all = sent_together((query_normed, pair_normed, rope_own), "sp", 0, 1)
    length = tokens * spread
    all_positions = jnp.arange(length, dtype=jnp.int32).astype(jnp.float32)

    def own_columns(weight, width):
        count = weight.shape[1] // (width * spread)
        return lax.dynamic_slice_in_dim(weight, device_index * count * width, count * width, 1)

    own_narrow_query = own_columns(narrow_query, width_narrow)
    own_broad_query = own_columns(broad_query, width_broad)
    own_narrow_key = own_columns(narrow_key, PLAIN_NARROW)
    own_narrow_value = own_columns(narrow_value, VALUE_SIZE)
    own_broad_key = own_columns(broad_key, PLAIN_BROAD)
    own_broad_value = own_columns(broad_value, VALUE_SIZE)
    query_sums = make_fold(
        query_all, sent_together((own_narrow_query, own_broad_query), "dp", 0, 1)
    )
    pair_sums = make_fold(
        pair_all,
        sent_together(
            (own_narrow_key, own_narrow_value, own_broad_key, own_broad_value), "dp", 0, 1
        ),
    )
    members = (
        arrange(query_sums[0], width_narrow, all_positions, 1, True),
        arrange(pair_sums[0], PLAIN_NARROW, all_positions, 1, False),
        arrange(pair_sums[1], VALUE_SIZE, all_positions, 1, False),
        arrange(query_sums[1], width_broad, all_positions, 1, True),
        arrange(pair_sums[2], PLAIN_BROAD, all_positions, 1, False),
        arrange(pair_sums[3], VALUE_SIZE, all_positions, 1, False),
    )
    mixed_first, mixed_second = attend_both(members, rope_all)
    back_first, back_second = sent_together_2((mixed_first, mixed_second), "sp", 0, 1, 2)
    return (finish(back_first), finish(back_second))


def solution(mesh):
    in_specs = (
        P("dp", "sp", None),
        P("dp", "sp", None),
        P("dp", "sp", None),
        P(),
        P(),
        P("dp", None),
        P("dp", None),
        P("dp", None),
        P("dp", None),
        P("dp", None),
        P("dp", None),
    )
    out_specs = (P("dp", "sp", None), P("dp", "sp", None))
    return jax.shard_map(
        on_device, mesh=mesh, in_specs=in_specs, out_specs=out_specs, check_vma=False
    )
```

profile of v0, /device:TPU:54, one launch (start us, length us, event | category | flops | bytes accessed | tf_op | source)
XLA Modules:
  0.0 213.9 jit_solution(568382685272743762)
XLA Ops:
  8.0 1.0 copy.44
  9.1 1.1 copy.43
  10.5 0.8 fusion.64
  11.3 0.9 fusion.60
  15.2 23.1 %all_gather.11 = bf16[512,320]{1,0:T(8,128)(2,1)S(1)} all-gather(bf16[16,320]{1,0:T(8,128)(2,1)S(1)} %pad_maximum_fusion.7), channel_id=1, replica_groups=mesh['sp'=16,'dp'=32] {'dp'}, dimensions={0}, use_global_device_ids=true | all-gather | bytes 337920 | tf_op jit(solution)/shard_map/all_gather | solution.py:19
  39.3 25.8 %all_gather.10 = bf16[768,256]{1,0:T(8,128)(2,1)} all-gather(bf16[24,256]{1,0:T(8,128)(2,1)S(1)} %pad_maximum_fusion.6), channel_id=1, replica_groups=mesh['sp'=16,'dp'=32] {'dp'}, dimensions={0}, use_global_device_ids=true | all-gather | bytes 405504 | tf_op jit(solution)/shard_map/all_gather | solution.py:19
  65.0 57.4 %all-gather.2.cloned.1.call-done = bf16[2048,1312]{0,1:T(8,128)(2,1)} async-done(((bf16[128,1312]{0,1:T(8,128)(2,1)}), bf16[2048,1312]{0,1:T(8,128)(2,1)}) %all-gather.2.cloned.1.call-update) | async-done | bytes 5373968 | tf_op jit(solution)/shard_map/all_gather | solution.py:19
  122.5 2.1 convolution_convert_fusion.1
  124.9 2.2 %convolution_convert_fusion.2 = bf16[2048,64]{0,1:T(8,128)(2,1)S(1)} fusion(bf16[2048,1312]{0,1:T(8,128)(2,1)} %all-gather.2.cloned.1.call-done, bf16[512,320]{1,0:T(8,128)(2,1)S(1)} %all_gather.11), kind=kOutput, calls=%fused_computation.36 | convolution fusion | flops 134348800 | bytes 2490368 | tf_op jit(solution)/shard_map/dot_general | solution.py:58
  127.3 0.9 split.48
  128.3 2.1 convolution_convert_fusion
  130.4 2.1 convolution_convert_fusion.3
  133.6 2.8 %fusion.46 = f32[2048,1,160]{0,2,1:T(8,128)S(1)} fusion(bf16[2048,1312]{0,1:T(8,128)(2,1)} %all-gather.2.cloned.1.call-done, bf16[768,256]{1,0:T(8,128)(2,1)} %all_gather.10), kind=kOutput, calls=%fused_computation.32 | convolution fusion | flops 503316480 | bytes 4849664 | tf_op jit(solution)/shard_map/dot_general | solution.py:58
  136.4 2.6 %fusion.49 = f32[2048,1,96]{0,2,1:T(8,128)S(1)} fusion(bf16[2048,1312]{0,1:T(8,128)(2,1)} %all-gather.2.cloned.1.call-done, bf16[768,256]{1,0:T(8,128)(2,1)S(1)} %copy-done.1), kind=kOutput, calls=%fused_computation.33 | convolution fusion | flops 301989888 | bytes 4128768 | tf_op jit(solution)/shard_map/dot_general | solution.py:58
  139.0 1.3 fusion.75
  140.3 1.0 copy.66
  141.3 1.0 copy.63
  142.3 1.9 copy.64
  144.2 1.9 copy.65
  146.0 1.8 pad_maximum_fusion.2
  147.9 10.5 %while.20 = (s32[]{:T(128)}, bf16[4,512,64]{1,2,0:T(8,128)(2,1)S(1)}, bf16[4,512,96]{2,1,0:T(8,128)(2,1)S(1)}, bf16[2048,96]{1,0:T(8,128)(2,1)S(1)}, bf16[2048,64]{1,0:T(8,128)(2,1)S(1)}, /*index=5*/s32[]{:T(128)}) while((s32[]{:T(128)}, bf16[4,512,64]{1,2,0:T(8,128)(2,1)S(1)}, bf16[4,512,96]{2,1,0:T(8,128)(2,1)S(1)}, ...), condition=%wide.region_5.6_spmd, body=%wide.region_2.5_spmd.sunk | while | flops 343997440 | bytes 13838421 | solution.py:89
  148.7 0.8 fusion.111
  149.5 1.0 fusion.112
  151.3 0.8 fusion.111
  152.1 1.0 fusion.112
  153.9 0.8 fusion.111
  154.8 1.0 fusion.112
  156.6 0.8 fusion.111
  157.4 1.0 fusion.112
  158.8 1.1 copy.68
  159.9 1.9 copy.67
  161.8 1.5 pad_maximum_fusion
  163.3 10.7 %while.21 = (s32[]{:T(128)}, bf16[4,512,64]{1,2,0:T(8,128)(2,1)S(1)}, bf16[4,512,160]{2,1,0:T(8,128)(2,1)S(1)}, bf16[2048,160]{1,0:T(8,128)(2,1)S(1)}, bf16[2048,64]{1,0:T(8,128)(2,1)S(1)}, /*index=5*/s32[]{:T(128)}) while((s32[]{:T(128)}, bf16[4,512,64]{1,2,0:T(8,128)(2,1)S(1)}, bf16[4,512,160]{2,1,0:T(8,128)(2,1)S(1)}, ...), condition=%wide.region_9.10_spmd, body=%wide.region_6.9_spmd.sunk | while | flops 478215168 | bytes 14493781 | solution.py:89
  163.4 0.8 multiply_reduce_fusion.7
  164.2 0.8 fusion.116
  165.0 1.0 fusion.117
  166.0 0.8 multiply_reduce_fusion.7
  166.9 0.8 fusion.116
  167.7 1.0 fusion.117
  168.7 0.8 multiply_reduce_fusion.7
  169.6 0.8 fusion.116
  170.4 1.0 fusion.117
  171.4 0.8 multiply_reduce_fusion.7
  172.2 0.8 fusion.116
  173.1 1.0 fusion.117
  176.0 27.2 %all_to_all.18 = bf16[16,2,8192]{2,1,0:T(2,128)(2,1)S(1)} all-to-all(bf16[16,2,8192]{2,1,0:T(2,128)(2,1)S(1)} %reshape.375), channel_id=1, replica_groups=mesh['sp'=16,'dp'=32] {'sp'}, dimensions={0} | all-to-all | bytes 1048576 | tf_op jit(solution)/shard_map/all_to_all | solution.py:26
  205.1 0.9 copy.62
  206.2 0.9 copy.61
  (55 shorter events, 14.4 us)
Async XLA Ops:
  7.2 31.9 %copy-start = (bf16[24,2560]{1,0:T(8,128)(2,1)S(1)}, bf16[24,2560]{1,0:T(8,128)(2,1)}, u32[]{:S(2)}) copy-start(bf16[24,2560]{1,0:T(8,128)(2,1)} %param.21) | copy-start | bytes 368644
  7.2 115.3 %all-gather.2.cloned.1.call-start = ((), (), s32[]{:S(2)}) async-start(), calls=%async_computation.1 | async-start | bytes 5709824 | tf_op jit(solution)/shard_map/all_gather | solution.py:19
  133.5 2.9 %copy-start.1 = (bf16[768,256]{1,0:T(8,128)(2,1)S(1)}, bf16[768,256]{1,0:T(8,128)(2,1)}, u32[]{:S(2)}) copy-start(bf16[768,256]{1,0:T(8,128)(2,1)} %all_gather.10) | copy-start | bytes 1179652
Sparse Core Ops, SparseCore 0:
  13.0 109.3 all-gather.1
where the time goes:
time: 215 us; the launch traced here: 214 us
  blocking collectives  76.1 us (35%)
  waiting for transfers between devices  57.4 us (27%)
  matrix products  28.3 us (13%)
  local copies, waits for them, and re-layouts  22.2 us (10%)
  other arithmetic  15.3 us (7%)
  between operations  14.3 us (7%)
    all_gather x1, waiting for transfers between devices, sent_together(): whole = lax.all_gather(both, axis, axis=dim, tiled=True)  57.4 us
    all_gather x2, blocking collectives, sent_together(): whole = lax.all_gather(both, axis, axis=dim, tiled=True)  48.8 us
    all_to_all x1, blocking collectives, sent_together_2(): lax.all_to_all(both, axis, split_axis=split_dim, concat_axis=concat_dim,...  27.2 us
    dot_general x6, matrix products, make_fold(): jnp.dot(latent, weight_rows, preferred_element_type=jnp.float32)  13.9 us
    concatenate x6, local copies, waits for them, and re-layouts, rotate(): jnp.concatenate([plain_part, first_half * cosine - second_half * sine_par...  8.72 us
    dot_general x8, matrix products, one_block(): jnp.dot(shifted.astype(jnp.bfloat16), value_head, preferred_element_type=...  7.89 us
    reduce_sum x8, other arithmetic, one_block(): totals = jnp.sum(shifted, axis=-1, keepdims=True)  6.59 us
    dot_general x8, matrix products, one_block(): jnp.einsum('qd,kd->qk', query_block, key_whole, preferred_element_type=jn...  6.55 us
  transfers between devices with their start and end apart: 1, of which 1 were waited for; matrix products, arithmetic and copies ran while one was open for 2% of the time, Pallas kernels for 0%

commit v1 on v0

v1 whole, which is shorter than its diff:
```python
import functools
import math

import jax
import jax.numpy as jnp
import numpy as np
from jax import lax
from jax.experimental import pallas as pl
from jax.experimental.pallas import tpu as pltpu
from jax.sharding import PartitionSpec as P

EPSILON = 1e-06
ROTARY_BASE = 10000.0
NZ = 16
NXY = 16
PXY = 4
PZ = 4
BF = jnp.bfloat16
F32 = jnp.float32
MESH = pl.DeviceIdType.MESH
NARROW_SCALE = 96 ** -0.5 * math.log2(math.e)
BROAD_SCALE = 160 ** -0.5 * math.log2(math.e)
KEY_BLOCK = 512


def rotary_tables():
    frequency = ROTARY_BASE ** (-np.arange(16, dtype=np.float64) / 16)
    lanes = np.tile(frequency, 8)
    coarse = (256.0 * np.arange(8))[:, None] * lanes[None, :]
    fine = np.arange(256.0)[:, None] * lanes[None, :]
    return tuple(
        np.asarray(t, np.float32)
        for t in (np.cos(coarse), np.sin(coarse), np.cos(fine), np.sin(fine))
    )


def lane_iota(shape):
    return lax.broadcasted_iota(jnp.int32, shape, len(shape) - 1)


def row_iota(shape):
    return lax.broadcasted_iota(jnp.int32, shape, 0)


def normalize(latent, gain_row):
    values = latent.astype(F32)
    scaled = values * lax.rsqrt(jnp.mean(values * values, axis=-1, keepdims=True) + EPSILON)
    return (scaled * gain_row).astype(BF)


def rotate(values, cosine, signed_sine):
    first = lane_iota(values.shape) % 32 < 16
    swapped = jnp.where(first, pltpu.roll(values, 112, 1), pltpu.roll(values, 16, 1))
    return values * cosine + swapped * signed_sine


def take(columns, segments):
    rows = columns.shape[0]
    lane = lane_iota((rows, 128))
    out, dest = None, 0
    for start, width in segments:
        tile, off = start // 128, start % 128
        span = 128 if off + width <= 128 else 256
        window = columns[:, tile * 128 : tile * 128 + span]
        shift = (dest - off) % span
        moved = pltpu.roll(window, shift, 1)[:, :128] if shift else window[:, :128]
        out = moved if out is None else jnp.where(lane >= dest, moved, out)
        dest += width
    return out


def ring_chip(ring, position):
    major = position // 4
    minor = lax.rem(position - major + 16, 4)
    return (minor, major) if ring == 0 else (major, minor)


def body(
    ql, kl, rk, qg, kg, ca, sa, cb, sb, nq, bq, nk, nv, bk, bv,
    out_n, out_b,
    raw_n, raw_b, wq8, wkv, kv, rt, qn, wq, wvt, qmt, kp, kr, vt, at, sbuf, cos_t, sin_t,
    in_sem, xy_send, xy_recv, dd_send, dd_recv, z_send, z_recv, zr_send, zr_recv,
    q_send, q_recv, o_send, o_recv,
):
    z = lax.axis_index("sp")
    d = lax.axis_index("dp")
    par = lax.rem(z, 2)
    core = lax.rem(d, 2)
    chip = d // 2
    cx, cy = lax.rem(chip, 4), chip // 4
    diag = lax.rem(cx + cy, 4)
    ring_pos = (4 * cy + diag, 4 * cx + diag)
    partner_core = d + 1 - 2 * core
    mate = z + 1 - 2 * par

    def slot_of(ring, position):
        x, y = ring_chip(ring, lax.rem(position + 32, 16))
        return (y * 4 + x) * 2 + core

    def cols(ref, width):
        return ref.at[:, pl.ds(pl.multiple_of(par * width, 128), width)]

    own_rows = pl.ds(pl.multiple_of(d * 16, 16), 16)
    loads = [
        pltpu.make_async_copy(cols(nq, 768), raw_n, in_sem.at[0]),
        pltpu.make_async_copy(cols(bq, 1280), raw_b, in_sem.at[1]),
        pltpu.make_async_copy(cols(nk, 512), wkv.at[own_rows, pl.ds(0, 512)], in_sem.at[2]),
        pltpu.make_async_copy(cols(bk, 1024), wkv.at[own_rows, pl.ds(512, 1024)], in_sem.at[3]),
        pltpu.make_async_copy(cols(nv, 512), wkv.at[own_rows, pl.ds(1536, 512)], in_sem.at[4]),
        pltpu.make_async_copy(cols(bv, 512), wkv.at[own_rows, pl.ds(2048, 512)], in_sem.at[5]),
    ]
    for load in loads:
        load.start()

    barrier = pltpu.get_barrier_semaphore()
    near = [{"sp": lax.rem(z + 1, 16)}, {"sp": lax.rem(z + 15, 16)}, {"dp": partner_core}]
    for ring in range(2):
        for step in (1, -1):
            near.append({"dp": slot_of(ring, ring_pos[ring] + step)})
    for who in near:
        pl.semaphore_signal(barrier, inc=1, device_id=who, device_id_type=MESH)

    kv[z] = normalize(kl[0], kg[...])
    half = pl.ds(pl.multiple_of(par * 128, 128), 128)
    coarse = pl.ds(z // 2, 1)
    cosine = ca[coarse, :] * cb[...] - sa[coarse, :] * sb[...]
    sine = sa[coarse, :] * cb[...] + ca[coarse, :] * sb[...]
    cos_t[...] = cosine
    sin_t[...] = jnp.where(lane_iota(sine.shape) % 32 < 16, -sine, sine)
    spread = (row_iota((32, 128)) == lane_iota((32, 128)) % 32).astype(BF)
    rope4 = jnp.dot(rk[0], spread, preferred_element_type=F32)
    rope4 = rotate(rope4, cos_t[half, :], sin_t[half, :])
    rt[z] = rope4.T[:32].astype(BF)
    qn[par] = normalize(ql[0], qg[...])
    for load in loads:
        load.wait()
    wn, wb = raw_n[...].astype(F32), raw_b[...].astype(F32)
    blocks = [take(wn, [(192 * j, 64), (192 * j + 96, 64)]) for j in range(4)]
    blocks += [take(wb, [(160 * h, 128)]) for h in range(8)]
    blocks += [take(wn, [(96 * h + 64, 32) for h in range(4 * g, 4 * g + 4)]) for g in range(2)]
    blocks += [take(wb, [(160 * h + 128, 32) for h in range(4 * g, 4 * g + 4)]) for g in range(2)]
    for i, block in enumerate(blocks):
        for t in range(3):
            wq8[3 * d + t, :, 128 * i : 128 * i + 128] = block[8 * t : 8 * t + 8].astype(BF)

    pl.semaphore_wait(barrier, 7)

    def unit(ring, slot):
        if ring == 0:
            return wq8.at[pl.ds(3 * slot, 3)]
        return wkv.at[pl.ds(pl.multiple_of(16 * slot, 16), 16)]

    def piece(ring, slot, i):
        if ring == 0:
            return wq8.at[pl.ds(3 * slot, 3), :, pl.ds(i * (2048 // PXY), 2048 // PXY)]
        rows = pl.ds(pl.multiple_of(16 * slot, 16), 16)
        return wkv.at[rows, pl.ds(i * (2560 // PXY), 2560 // PXY)]

    def xy_copy(ring, way, step, i):
        sign = 1 - 2 * way
        slot = slot_of(ring, ring_pos[ring] - sign * (step - 1))
        ref = piece(ring, slot, i)
        flow = 2 * ring + way
        index = (step - 1) * PXY + i
        to = slot_of(ring, ring_pos[ring] + sign)
        return pltpu.make_async_remote_copy(
            ref, ref, xy_send.at[flow, index], xy_recv.at[flow, index],
            device_id={"dp": to}, device_id_type=MESH,
        )

    def xy_landed(ring, way, step, i):
        sign = 1 - 2 * way
        slot = slot_of(ring, ring_pos[ring] - sign * step)
        ref = piece(ring, slot, i)
        flow = 2 * ring + way
        index = (step - 1) * PXY + i
        pltpu.make_async_remote_copy(
            ref, ref, xy_send.at[flow, index], xy_recv.at[flow, index],
            device_id={"dp": d}, device_id_type=MESH,
        ).wait_recv()

    def dd_copy(ring, offset):
        slot = slot_of(ring, ring_pos[ring] + offset)
        ref = unit(ring, slot)
        index = offset + 7
        return pltpu.make_async_remote_copy(
            ref, ref, dd_send.at[ring, index], dd_recv.at[ring, index],
            device_id={"dp": partner_core}, device_id_type=MESH,
        )

    def dd_landed(ring, offset):
        x, y = ring_chip(ring, lax.rem(ring_pos[ring] + offset + 32, 16))
        ref = unit(ring, (y * 4 + x) * 2 + 1 - core)
        index = offset + 7
        pltpu.make_async_remote_copy(
            ref, ref, dd_send.at[ring, index], dd_recv.at[ring, index],
            device_id={"dp": partner_core}, device_id_type=MESH,
        ).wait_recv()

    rows_z = 128 // PZ

    def z_ref(slot, i):
        return rt.at[slot] if i == PZ else kv.at[slot, pl.ds(i * rows_z, rows_z)]

    def z_desc(way, step, i, slot):
        ref = z_ref(slot, i)
        sign = 1 - 2 * way
        index = (step - 1) * (PZ + 1) + i
        return pltpu.make_async_remote_copy(
            ref, ref, z_send.at[way, index], z_recv.at[way, index],
            device_id={"sp": lax.rem(z + sign + 16, 16)}, device_id_type=MESH,
        )

    def z_copy(way, step, i):
        return z_desc(way, step, i, lax.rem(z - (1 - 2 * way) * (step - 1) + 32, 16))

    def z_landed(way, step, i):
        z_desc(way, step, i, lax.rem(z - (1 - 2 * way) * step + 32, 16)).wait_recv()

    def xy_pieces(way, step):
        if step < 8:
            return list(range(PXY))
        return list(range(PXY // 2)) if way == 0 else list(range(PXY // 2, PXY))

    def z_pieces(way, step):
        if step < 8:
            return [PZ] + list(range(PZ))
        return [PZ] + list(range(PZ // 2)) if way == 0 else list(range(PZ // 2, PZ))

    started = []

    def start(copy):
        copy.start()
        started.append(copy)

    for i in range(PXY):
        for ring in range(2):
            for way in range(2):
                start(xy_copy(ring, way, 1, i))
    for i in z_pieces(0, 1):
        for way in range(2):
            start(z_copy(way, 1, i))
    for ring in range(2):
        start(dd_copy(ring, 0))
    mine = qn.at[par]
    q_copy = pltpu.make_async_remote_copy(
        mine, mine, q_send.at[0], q_recv.at[0], device_id={"sp": mate}, device_id_type=MESH
    )
    start(q_copy)

    def xy_event(step, i):
        for ring in range(2):
            for way in range(2):
                if i not in xy_pieces(way, step):
                    continue
                xy_landed(ring, way, step, i)
                if step < 8 and i in xy_pieces(way, step + 1):
                    start(xy_copy(ring, way, step + 1, i))
                if step < 8 and i == PXY - 1:
                    start(dd_copy(ring, (2 * way - 1) * step))
            if step == 8 and i == PXY - 1:
                start(dd_copy(ring, 8))

    def z_event(step, i):
        for way in range(2):
            if i not in z_pieces(way, step):
                continue
            z_landed(way, step, i)
            if step < 8 and i in z_pieces(way, step + 1):
                start(z_copy(way, step + 1, i))

    events = []
    for step in range(1, 9):
        for i in range(PXY):
            events.append((2.1 * (step - 1) + 2.1 * (i + 1) / PXY, xy_event, step, i))
        events.append((3.0 * (step - 1) + 0.2, z_event, step, PZ))
        for i in range(PZ):
            events.append((3.0 * (step - 1) + 3.0 * (i + 1) / PZ, z_event, step, i))
    for _, event, step, i in sorted(events, key=lambda e: e[0]):
        event(step, i)
    for ring in range(2):
        for offset in range(-7, 9):
            dd_landed(ring, offset)
    theirs = qn.at[1 - par]
    pltpu.make_async_remote_copy(
        theirs, theirs, q_send.at[0], q_recv.at[0], device_id={"sp": mate}, device_id_type=MESH
    ).wait_recv()

    def pack_rows(g, carry):
        pair = jnp.concatenate([wq8[2 * g].astype(F32), wq8[2 * g + 1].astype(F32)], axis=0)
        wq[pl.ds(pl.multiple_of(16 * g, 16), 16), :] = pair.astype(BF)
        return carry

    lax.fori_loop(0, 48, pack_rows, 0)
    for i in range(8):
        wvt[128 * i : 128 * i + 128, :] = wkv[:, 1536 + 128 * i : 1664 + 128 * i].T

    tokens = jnp.concatenate([qn[0], qn[1]], axis=0)
    group = row_iota((128, 256)) // 32
    side = row_iota((128, 256)) // 64
    nothing = jnp.zeros((128, 256), BF)
    for pair in range(8):
        both = jnp.dot(tokens, wq[:, 256 * pair : 256 * pair + 256], preferred_element_type=F32)
        for k in range(2):
            block = 2 * pair + k
            part = both[:, 128 * k : 128 * k + 128]
            if block >= 12:
                part = rotate(part, cos_t[...], sin_t[...])
            turned = part.astype(BF).T
            if block < 4:
                for s in range(2):
                    qmt[2 * block + s, 0:128, :] = jnp.where(side == s, turned, nothing)
            elif block < 12:
                qmt[block + 4, 0:128, :] = turned
            else:
                for g in range(4):
                    head = 4 * (block - 12) + g
                    qmt[head, 128:256, :] = jnp.where(group == g, turned, nothing)

    for h in range(16):
        vt[h, 64:80, :] = jnp.ones((16, 2048), BF)

    def project(b, carry):
        rows = pl.ds(pl.multiple_of(256 * b, 256), 256)
        x = jnp.concatenate([kv[2 * b], kv[2 * b + 1]], axis=0)
        for i in range(6):
            kp[rows, 256 * i : 256 * i + 256] = jnp.dot(
                x, wkv[:, 256 * i : 256 * i + 256], preferred_element_type=F32
            ).astype(BF)
        for i in range(4):
            turned = lax.dot_general(
                wvt[256 * i : 256 * i + 256, :], x, (((1,), (1,)), ((), ())),
                preferred_element_type=F32,
            ).astype(BF)
            for k in range(4):
                vt[4 * i + k, 0:64, rows] = turned[64 * k : 64 * k + 64]
        for k in range(2):
            one = rt[2 * b + k].astype(F32)
            kr[pl.ds(pl.multiple_of(256 * b + 128 * k, 128), 128), :] = (
                jnp.concatenate([one, one, one, one], axis=0).T.astype(BF)
            )
        return carry

    lax.fori_loop(0, 8, project, 0)

    def attend(h, factor, column):
        top = jnp.full((1, 256), -1e30, F32)
        total = jnp.zeros((80, 256), F32)
        operand = qmt[h]
        for b in range(2048 // KEY_BLOCK):
            rows = slice(b * KEY_BLOCK, (b + 1) * KEY_BLOCK)
            keys = jnp.concatenate([kp[rows, pl.ds(column, 128)], kr[rows, :]], axis=1)
            scores = jnp.dot(keys, operand, preferred_element_type=F32)
            new_top = jnp.maximum(top, jnp.max(scores, axis=0, keepdims=True))
            weights = jnp.exp2((scores - new_top) * factor).astype(BF)
            total = total * jnp.exp2((top - new_top) * factor) + jnp.dot(
                vt[h, :, rows], weights, preferred_element_type=F32
            )
            top = new_top
        return total[0:64] / total[64:65]

    def out_desc(j):
        broad = j // 4
        dst = 8 * broad + 4 * par + j - 4 * broad
        return pltpu.make_async_remote_copy(
            sbuf.at[j], at.at[dst], o_send.at[j], o_recv.at[j],
            device_id={"sp": mate}, device_id_type=MESH,
        )

    def two_heads(j, carry):
        broad = j // 4
        factor = jnp.where(broad == 0, NARROW_SCALE, BROAD_SCALE).astype(F32)
        parts = []
        for k in range(2):
            h = 2 * j + k
            block = (1 - broad) * j + broad * (h - 4)
            parts.append(attend(h, factor, pl.multiple_of(block * 128, 128)))
        stacked = jnp.concatenate(parts, axis=0).astype(BF)
        low, high = stacked[:, 0:128].T, stacked[:, 128:256].T
        even = par == 0
        at[8 * broad + 4 * par + j - 4 * broad] = jnp.where(even, low, high)
        sbuf[j] = jnp.where(even, high, low)
        out_desc(j).start()
        return carry

    lax.fori_loop(0, 8, two_heads, 0)

    def landed(j, carry):
        broad = j // 4
        src = 8 * broad + 4 * (1 - par) + j - 4 * broad
        pltpu.make_async_remote_copy(
            at.at[src], at.at[src], o_send.at[j], o_recv.at[j],
            device_id={"sp": mate}, device_id_type=MESH,
        ).wait_recv()
        out_desc(j).wait_send()
        return carry

    lax.fori_loop(0, 8, landed, 0)
    for which, out in enumerate((out_n, out_b)):
        values = [at[8 * which + i].astype(F32) for i in range(8)]
        squares = sum(v * v for v in values)
        mean = jnp.sum(squares, axis=-1, keepdims=True) * (1.0 / 1024)
        scale = lax.rsqrt(mean + EPSILON)
        for i in range(8):
            out[0, :, 128 * i : 128 * i + 128] = (values[i] * scale).astype(BF)

    for copy in started:
        copy.wait_send()


def on_device(ql, kl, rk, qg, kg, nq, bq, nk, nv, bk, bv):
    vmem = pl.BlockSpec(memory_space=pltpu.VMEM)
    hbm = pl.BlockSpec(memory_space=pl.ANY)
    dma = pltpu.SemaphoreType.DMA
    return pl.pallas_call(
        body,
        out_shape=[jax.ShapeDtypeStruct((1, 128, 1024), BF)] * 2,
        in_specs=[vmem] * 9 + [hbm] * 6,
        out_specs=[vmem] * 2,
        scratch_shapes=[
            pltpu.VMEM((24, 768), BF),
            pltpu.VMEM((24, 1280), BF),
            pltpu.VMEM((96, 8, 2048), BF),
            pltpu.VMEM((512, 2560), BF),
            pltpu.VMEM((16, 128, 512), BF),
            pltpu.VMEM((16, 32, 128), BF),
            pltpu.VMEM((2, 128, 768), BF),
            pltpu.VMEM((768, 2048), BF),
            pltpu.VMEM((1024, 512), BF),
            pltpu.VMEM((16, 256, 256), BF),
            pltpu.VMEM((2048, 1536), BF),
            pltpu.VMEM((2048, 128), BF),
            pltpu.VMEM((16, 80, 2048), BF),
            pltpu.VMEM((16, 128, 128), BF),
            pltpu.VMEM((8, 128, 128), BF),
            pltpu.VMEM((256, 128), F32),
            pltpu.VMEM((256, 128), F32),
            dma((6,)),
            dma((4, 8 * PXY)),
            dma((4, 8 * PXY)),
            dma((2, 16)),
            dma((2, 16)),
            dma((2, 8 * (PZ + 1))),
            dma((2, 8 * (PZ + 1))),
            dma((1,)),
            dma((1,)),
            dma((1,)),
            dma((1,)),
            dma((8,)),
            dma((8,)),
        ],
        compiler_params=pltpu.CompilerParams(
            collective_id=0, has_side_effects=True, vmem_limit_bytes=60 * 1024 * 1024
        ),
        name="latent_attention",
    )(
        ql, kl, rk, qg.reshape(1, -1), kg.reshape(1, -1),
        *(jnp.asarray(t) for t in rotary_tables()),
        nq, bq, nk, nv, bk, bv,
    )


def solution(mesh):
    in_specs = (
        P("dp", "sp", None),
        P("dp", "sp", None),
        P("dp", "sp", None),
        P(),
        P(),
        P("dp", None),
        P("dp", None),
        P("dp", None),
        P("dp", None),
        P("dp", None),
        P("dp", None),
    )
    out_specs = (P("dp", "sp", None), P("dp", "sp", None))
    return jax.shard_map(
        on_device, mesh=mesh, in_specs=in_specs, out_specs=out_specs, check_vma=False
    )
```

time: 215 us -> 99.3 us (0.46)
  the two profiles are of different devices: /device:TPU:54 before, /device:TPU:32 now
where the time goes in v1:
time: 99.3 us; the launch traced here: 99 us
  Pallas kernels  94 us (95%)
  local copies, waits for them, and re-layouts  4.42 us (4%)
    pallas_call x1, Pallas kernels, on_device(): pl.pallas_call(body, out_shape=[jax.ShapeDtypeStruct((1, 128, 1024), BF)]...  94 us
    unnamed x7, local copies, waits for them, and re-layouts  3.14 us

profile of v1, /device:TPU:32, one launch (start us, length us, event | category | flops | bytes accessed | tf_op | source)
XLA Modules:
  0.0 99.0 jit_solution(13423855480166894517)
XLA Ops:
  0.6 0.0 copy-start.1
  0.6 1.3 %reshape.10.qg = f32[1,768]{1,0:T(1,128)} reshape(f32[768]{0:T(1024)} %param.18) | data formatting | bytes 6144 | tf_op jit(solution)/shard_map/reshape | solution.py:457
  1.9 0.0 copy-done.1
  1.9 0.7 copy.17.rk
  2.6 94.0 %latent_attention.1 = (bf16[1,128,1024]{2,1,0:T(8,128)(2,1)}, bf16[1,128,1024]{2,1,0:T(8,128)(2,1)}) custom-call(bf16[1,128,768]{2,1,0:T(8,128)(2,1)} %ql.1, bf16[1,128,512]{2,1,0:T(8,128)(2,1)} %kl.1, bf16[1,128,32]{2,1,0:T(8,128)(2,1)} %copy.17.rk, f32[1,768]{1,0:T(1,128)} %reshape.10.qg, f32[1,512]{1,0:T(1,128)} %bitcast.1, f32[8,128]{1,0:T(8,128)} %constant.8.clone.ca, ...), custom_call_target="tpu_custom_call" | custom-call | tf_op jit(solution)/shard_map/latent_attention/pallas_call | solution.py:415
  96.6 0.0 copy-start
  96.6 1.7 %copy.20 = bf16[1,128,1024]{2,1,0:T(8,128)(2,1)} copy(bf16[1,128,1024]{2,1,0:T(8,128)(2,1)} %get-tuple-element.4) | data formatting | bytes 524288
  98.3 0.0 copy-done
  98.3 0.7 copy.21
Async XLA Ops:
  0.6 1.3 %copy-start.1 = (bf16[1,128,32]{1,2,0:T(8,128)(2,1)S(1)}, bf16[1,128,32]{1,2,0:T(8,128)(2,1)}, u32[]{:S(2)}) copy-start(bf16[1,128,32]{1,2,0:T(8,128)(2,1)} %param.17) | copy-start | bytes 24580
  96.6 1.7 %copy-start = (bf16[1,128,1024]{2,1,0:T(8,128)(2,1)S(1)}, bf16[1,128,1024]{2,1,0:T(8,128)(2,1)}, u32[]{:S(2)}) copy-start(bf16[1,128,1024]{2,1,0:T(8,128)(2,1)} %get-tuple-element.5) | copy-start | bytes 786436

commit v2 on v1

v2 whole, which is shorter than its diff:
```python
import functools
import math

import jax
import jax.numpy as jnp
import numpy as np
from jax import lax
from jax.experimental import pallas as pl
from jax.experimental.pallas import tpu as pltpu
from jax.sharding import PartitionSpec as P

EPSILON = 1e-06
ROTARY_BASE = 10000.0
PZ = 4
Z_EARLY = 4
HOOK = 4
BF = jnp.bfloat16
F32 = jnp.float32
MESH = pl.DeviceIdType.MESH
NARROW_SCALE = 96 ** -0.5 * math.log2(math.e)
BROAD_SCALE = 160 ** -0.5 * math.log2(math.e)


def rotary_tables():
    frequency = ROTARY_BASE ** (-np.arange(16, dtype=np.float64) / 16)
    lanes = np.tile(frequency, 8)
    coarse = (256.0 * np.arange(8))[:, None] * lanes[None, :]
    fine = np.arange(256.0)[:, None] * lanes[None, :]
    return tuple(
        np.asarray(t, np.float32)
        for t in (np.cos(coarse), np.sin(coarse), np.cos(fine), np.sin(fine))
    )


def lane_iota(shape):
    return lax.broadcasted_iota(jnp.int32, shape, len(shape) - 1)


def row_iota(shape):
    return lax.broadcasted_iota(jnp.int32, shape, 0)


def normalize(latent, gain_row):
    values = latent.astype(F32)
    scaled = values * lax.rsqrt(jnp.mean(values * values, axis=-1, keepdims=True) + EPSILON)
    return (scaled * gain_row).astype(BF)


def rotate(values, cosine, signed_sine):
    first = lane_iota(values.shape) % 32 < 16
    swapped = jnp.where(first, pltpu.roll(values, 112, 1), pltpu.roll(values, 16, 1))
    return values * cosine + swapped * signed_sine


def take(columns, segments):
    rows = columns.shape[0]
    lane = lane_iota((rows, 128))
    out, dest = None, 0
    for start, width in segments:
        tile, off = start // 128, start % 128
        span = 128 if off + width <= 128 else 256
        window = columns[:, tile * 128 : tile * 128 + span]
        shift = (dest - off) % span
        moved = pltpu.roll(window, shift, 1)[:, :128] if shift else window[:, :128]
        out = moved if out is None else jnp.where(lane >= dest, moved, out)
        dest += width
    return out


def body(
    ql, kl, rk, qg, kg, ca, sa, cb, sb, nq, bq, nk, nv, bk, bv,
    out_n, out_b,
    raw_n, raw_b, wq8, wkv, kv, rt, qn, wq, wvt, qmt, kp, kr, vt, at, sbuf, cos_t, sin_t,
    s_buf, p_buf, acc_buf, top_buf,
    in_sem, f_send, f_recv, g_send, g_recv, dd_send, dd_recv, z_send, z_recv,
    q_send, q_recv, o_send, o_recv,
):
    z = lax.axis_index("sp")
    d = lax.axis_index("dp")
    par = lax.rem(z, 2)
    core = lax.rem(d, 2)
    chip = d // 2
    here = (lax.rem(chip, 4), chip // 4)
    partner_core = d + 1 - 2 * core
    mate = z + 1 - 2 * par
    zs = {k: lax.rem(z + k + 16, 16) for k in range(-8, 9)}

    where = {}
    for t in range(2):
        along = [[lax.rem(here[axis] + k, 4) for k in range(4)] for axis in (t, 1 - t)]
        for a in range(4):
            for b in range(4):
                xy = (along[0][a], along[1][b]) if t == 0 else (along[1][b], along[0][a])
                where[t, a, b] = (xy[1] * 4 + xy[0]) * 2 + core

    def cols(ref, width):
        return ref.at[:, pl.ds(pl.multiple_of(par * width, 128), width)]

    own_rows = pl.ds(pl.multiple_of(d * 16, 16), 16)
    loads = [
        pltpu.make_async_copy(cols(nq, 768), raw_n, in_sem.at[0]),
        pltpu.make_async_copy(cols(bq, 1280), raw_b, in_sem.at[1]),
        pltpu.make_async_copy(cols(nk, 512), wkv.at[own_rows, pl.ds(0, 512)], in_sem.at[2]),
        pltpu.make_async_copy(cols(bk, 1024), wkv.at[own_rows, pl.ds(512, 1024)], in_sem.at[3]),
        pltpu.make_async_copy(cols(nv, 512), wkv.at[own_rows, pl.ds(1536, 512)], in_sem.at[4]),
        pltpu.make_async_copy(cols(bv, 512), wkv.at[own_rows, pl.ds(2048, 512)], in_sem.at[5]),
    ]
    for load in loads:
        load.start()

    barrier = pltpu.get_barrier_semaphore()
    near = [{"sp": zs[1]}, {"sp": zs[-1]}, {"dp": partner_core}]
    near += [{"dp": where[t, k, 0]} for t in range(2) for k in (1, 3)]
    for who in near:
        pl.semaphore_signal(barrier, inc=1, device_id=who, device_id_type=MESH)

    kv[z] = normalize(kl[0], kg[...])
    half = pl.ds(pl.multiple_of(par * 128, 128), 128)
    coarse = pl.ds(z // 2, 1)
    cosine = ca[coarse, :] * cb[...] - sa[coarse, :] * sb[...]
    sine = sa[coarse, :] * cb[...] + ca[coarse, :] * sb[...]
    cos_t[...] = cosine
    sin_t[...] = jnp.where(lane_iota(sine.shape) % 32 < 16, -sine, sine)
    own_rope = rk[0].astype(F32)
    rope4 = jnp.concatenate([own_rope] * 4, axis=0).T
    rope4 = rotate(rope4, cos_t[half, :], sin_t[half, :])
    rt[z] = rope4.T[:32].astype(BF)
    qn[par] = normalize(ql[0], qg[...])
    for load in loads:
        load.wait()
    wn, wb = raw_n[...].astype(F32), raw_b[...].astype(F32)
    blocks = [take(wn, [(192 * j, 64), (192 * j + 96, 64)]) for j in range(4)]
    blocks += [take(wb, [(160 * h, 128)]) for h in range(8)]
    blocks += [take(wn, [(96 * h + 64, 32) for h in range(4 * g, 4 * g + 4)]) for g in range(2)]
    blocks += [take(wb, [(160 * h + 128, 32) for h in range(4 * g, 4 * g + 4)]) for g in range(2)]
    for i, block in enumerate(blocks):
        for t in range(3):
            wq8[3 * d + t, :, 128 * i : 128 * i + 128] = block[8 * t : 8 * t + 8].astype(BF)

    pl.semaphore_wait(barrier, 7)

    started = []

    def start(make):
        make().start()
        started.append(make)

    def piece(t, slot, h):
        if t == 0:
            return wq8.at[pl.ds(3 * slot, 3), :, pl.ds(h * 1024, 1024)]
        return wkv.at[pl.ds(pl.multiple_of(16 * slot, 16), 16), pl.ds(h * 1280, 1280)]

    def xy_desc(t, a, b, h, send, recv, to):
        ref = piece(t, where[t, a, b], h)
        return pltpu.make_async_remote_copy(
            ref, ref, send, recv, device_id={"dp": to}, device_id_type=MESH
        )

    def f_send_copy(t, a, h, to):
        named = (a - to) % 4
        index = (t * 4 + named) * 2 + h
        return lambda: xy_desc(
            t, a, 0, h, f_send.at[index], f_recv.at[index], where[t, to % 4, 0]
        )

    def g_send_copy(t, a, b, h, to):
        named = (b - to) % 4
        index = ((t * 4 + a) * 4 + named) * 2 + h
        return lambda: xy_desc(
            t, a, b, h, g_send.at[index], g_recv.at[index], where[t, 0, to % 4]
        )

    def d_copy(t, a, b, h):
        index = ((t * 4 + a) * 4 + b) * 2 + h
        return lambda: xy_desc(
            t, a, b, h, dd_send.at[index], dd_recv.at[index], partner_core
        )

    def column(t, a, h):
        for to in (1, -1):
            start(g_send_copy(t, a, 0, h, to))
        start(d_copy(t, a, 0, h))

    def f_event(t, a, h):
        index = (t * 4 + a) * 2 + h
        xy_desc(t, a, 0, h, f_send.at[index], f_recv.at[index], d).wait_recv()
        if (a, h) == (3, 0):
            start(f_send_copy(t, a, h, 1))
        if (a, h) == (1, 1):
            start(f_send_copy(t, a, h, -1))
        column(t, a, h)

    def g_event(t, a, b, h):
        index = ((t * 4 + a) * 4 + b) * 2 + h
        xy_desc(t, a, b, h, g_send.at[index], g_recv.at[index], d).wait_recv()
        if (b, h) == (3, 0):
            start(g_send_copy(t, a, b, h, 1))
        if (b, h) == (1, 1):
            start(g_send_copy(t, a, b, h, -1))
        start(d_copy(t, a, b, h))

    rows_z = 128 // PZ

    def z_desc(way, step, i, slot):
        ref = rt.at[slot] if i == PZ else kv.at[slot, pl.ds(i * rows_z, rows_z)]
        index = (step - 1) * (PZ + 1) + i
        return pltpu.make_async_remote_copy(
            ref, ref, z_send.at[way, index], z_recv.at[way, index],
            device_id={"sp": zs[1 - 2 * way]}, device_id_type=MESH,
        )

    def z_copy(way, step, i):
        return lambda: z_desc(way, step, i, zs[-(1 - 2 * way) * (step - 1)])

    def z_pieces(way, step):
        if step < 8:
            return [PZ] + list(range(PZ))
        return [PZ] + list(range(PZ // 2)) if way == 0 else list(range(PZ // 2, PZ))

    def z_event(step, i):
        for way in range(2):
            if i not in z_pieces(way, step):
                continue
            z_desc(way, step, i, zs[-(1 - 2 * way) * step]).wait_recv()
            if step < 8 and i in z_pieces(way, step + 1):
                start(z_copy(way, step + 1, i))

    def z_step(step):
        for i in z_pieces(0, 1):
            z_event(step, i)

    for h in range(2):
        for t in (1, 0):
            for to in (1, -1):
                start(f_send_copy(t, 0, h, to))
    for i in z_pieces(0, 1):
        for way in range(2):
            start(z_copy(way, 1, i))
    for h in range(2):
        for t in (1, 0):
            column(t, 0, h)
    mine = qn.at[par]
    start(
        lambda: pltpu.make_async_remote_copy(
            mine, mine, q_send.at[0], q_recv.at[0], device_id={"sp": mate}, device_id_type=MESH
        )
    )

    events = []
    for t in (1, 0):
        for h in range(2):
            for a in (1, 3):
                events.append((3.0 + h, f_event, (t, a, h)))
            events.append((6.0 + h, f_event, (t, 2, h)))
            for b in (1, 3):
                events.append((5.0 + h, g_event, (t, 0, b, h)))
                events.append((8.0 + h, g_event, (t, 1, b, h)))
                events.append((10.0 + h, g_event, (t, 3, b, h)))
                events.append((13.0 + h, g_event, (t, 2, b, h)))
            events.append((8.5 + h, g_event, (t, 0, 2, h)))
            events.append((11.5 + h, g_event, (t, 1, 2, h)))
            events.append((13.5 + h, g_event, (t, 3, 2, h)))
            events.append((16.5 + h, g_event, (t, 2, 2, h)))
    for step in range(1, Z_EARLY + 1):
        for k, i in enumerate(z_pieces(0, 1)):
            events.append((3.7 * step - 2 + 0.5 * k, z_event, (step, i)))
    for _, event, what in sorted(events, key=lambda e: e[0]):
        event(*what)
    for t in (1, 0):
        for a in range(4):
            for b in range(4):
                for h in range(2):
                    index = ((t * 4 + a) * 4 + b) * 2 + h
                    ref = piece(t, where[t, a, b] + 1 - 2 * core, h)
                    pltpu.make_async_remote_copy(
                        ref, ref, dd_send.at[index], dd_recv.at[index],
                        device_id={"dp": partner_core}, device_id_type=MESH,
                    ).wait_recv()
    theirs = qn.at[1 - par]
    pltpu.make_async_remote_copy(
        theirs, theirs, q_send.at[0], q_recv.at[0], device_id={"sp": mate}, device_id_type=MESH
    ).wait_recv()

    def pack_rows(g, carry):
        pair = jnp.concatenate([wq8[2 * g].astype(F32), wq8[2 * g + 1].astype(F32)], axis=0)
        wq[pl.ds(pl.multiple_of(16 * g, 16), 16), :] = pair.astype(BF)
        return carry

    lax.fori_loop(0, 48, pack_rows, 0)
    for i in range(8):
        wvt[128 * i : 128 * i + 128, :] = wkv[:, 1536 + 128 * i : 1664 + 128 * i].T

    tokens = jnp.concatenate([qn[0], qn[1]], axis=0)
    group = row_iota((128, 256)) // 32
    side = row_iota((128, 256)) // 64
    nothing = jnp.zeros((128, 256), BF)
    for pair in range(8):
        both = jnp.dot(tokens, wq[:, 256 * pair : 256 * pair + 256], preferred_element_type=F32)
        for k in range(2):
            block = 2 * pair + k
            part = both[:, 128 * k : 128 * k + 128]
            if block >= 12:
                part = rotate(part, cos_t[...], sin_t[...])
            turned = part.astype(BF).T
            if block < 4:
                for s in range(2):
                    qmt[2 * block + s, 0:128, :] = jnp.where(side == s, turned, nothing)
            elif block < 12:
                qmt[block + 4, 0:128, :] = turned
            else:
                for g in range(4):
                    head = 4 * (block - 12) + g
                    qmt[head, 128:256, :] = jnp.where(group == g, turned, nothing)

    for h in range(16):
        vt[h, 64:80, :] = jnp.ones((16, 2048), BF)

    def project(b, one, two):
        rows = pl.ds(pl.multiple_of(256 * b, 256), 256)
        x = jnp.concatenate([kv[one], kv[two]], axis=0)
        for i in range(6):
            kp[rows, 256 * i : 256 * i + 256] = jnp.dot(
                x, wkv[:, 256 * i : 256 * i + 256], preferred_element_type=F32
            ).astype(BF)
        for i in range(4):
            turned = lax.dot_general(
                wvt[256 * i : 256 * i + 256, :], x, (((1,), (1,)), ((), ())),
                preferred_element_type=F32,
            ).astype(BF)
            for k in range(4):
                vt[4 * i + k, 0:64, rows] = turned[64 * k : 64 * k + 64]
        for k, slot in enumerate((one, two)):
            own = rt[slot].astype(F32)
            kr[pl.ds(pl.multiple_of(256 * b + 128 * k, 128), 128), :] = (
                jnp.concatenate([own, own, own, own], axis=0).T.astype(BF)
            )

    def project_steps(first, last):
        def one_step(s, carry):
            project(s - 1, lax.rem(z + 16 - s, 16), lax.rem(z + lax.rem(s, 8) + 16, 16))
            return carry

        lax.fori_loop(first, last + 1, one_step, 0)

    def out_desc(j):
        broad = j // 4
        dst = 8 * broad + 4 * par + j - 4 * broad
        return pltpu.make_async_remote_copy(
            sbuf.at[j], at.at[dst], o_send.at[j], o_recv.at[j],
            device_id={"sp": mate}, device_id_type=MESH,
        )

    def finish_pair(j, parts):
        broad = j // 4
        stacked = jnp.concatenate(parts, axis=0).astype(BF)
        low, high = stacked[:, 0:128].T, stacked[:, 128:256].T
        even = par == 0
        at[8 * broad + 4 * par + j - 4 * broad] = jnp.where(even, low, high)
        sbuf[j] = jnp.where(even, high, low)
        out_desc(j).start()

    def factor_of(h):
        return jnp.where(h < 8, NARROW_SCALE, BROAD_SCALE).astype(F32)

    def attention(block0, count, last, hook):
        def rows_of(b):
            return slice((block0 + b) * 256, (block0 + b) * 256 + 256)

        def here_of(b):
            return slice(b * 256, b * 256 + 256)

        def score(h, slot, b):
            broad = h // 8
            block = (1 - broad) * (h // 2) + broad * (h - 4)
            lanes = pl.ds(pl.multiple_of(block * 128, 128), 128)
            keys = jnp.concatenate([kp[rows_of(b), lanes], kr[rows_of(b), :]], axis=1)
            scores = jnp.dot(keys, qmt[h], preferred_element_type=F32)
            s_buf[slot, here_of(b), :] = scores
            return jnp.max(scores.reshape(32, 8, 256), axis=0)

        def settle(h, peak):
            top = jnp.max(peak, axis=0, keepdims=True)
            if last:
                top = jnp.maximum(top, top_buf[0, h])
            top_buf[int(last), h] = top
            return top

        def soften(slot, b, top, factor):
            p_buf[slot, here_of(b), :] = jnp.exp2(
                (s_buf[slot, here_of(b), :] - top) * factor
            ).astype(BF)

        def gather(h, slot):
            keys = slice(block0 * 256, (block0 + count) * 256)
            return jnp.dot(
                vt[h, :, keys], p_buf[slot, : count * 256, :], preferred_element_type=F32
            )

        def all_scores(h, slot):
            peak = score(h, slot, 0)
            for b in range(1, count):
                peak = jnp.maximum(peak, score(h, slot, b))
            return settle(h, peak)

        first_top = all_scores(0, 0)
        for b in range(count):
            soften(0, b, first_top, factor_of(0))
        second_top = all_scores(1, 1)

        def step(i, top):
            hook(i)
            parts = []
            for k in range(2):
                h = 2 * i + k
                ahead = jnp.minimum(h + 2, 15)
                factor = factor_of(jnp.minimum(h + 1, 15))
                sums = gather(h, k)
                peak = None
                for b in range(count):
                    found = score(ahead, k, b)
                    peak = found if peak is None else jnp.maximum(peak, found)
                    soften(1 - k, b, top, factor)
                if last:
                    kept = jnp.exp2((top_buf[0, h] - top_buf[1, h]) * factor_of(h))
                    whole = acc_buf[h] * kept + sums
                    parts.append(whole[0:64] / whole[64:65])
                else:
                    acc_buf[h] = sums
                top = settle(ahead, peak)
            if last:
                finish_pair(i, parts)
            return top

        lax.fori_loop(0, 8, step, second_top)

    for step in range(Z_EARLY + 1, 6):
        z_step(step)
    project_steps(1, 5)
    z_step(6)

    def hook(i):
        @pl.when(i == HOOK)
        def _():
            z_step(7)

    attention(0, 5, False, hook)
    z_step(8)
    project_steps(6, 8)
    attention(5, 3, True, lambda i: None)

    def landed(j, carry):
        broad = j // 4
        src = 8 * broad + 4 * (1 - par) + j - 4 * broad
        pltpu.make_async_remote_copy(
            at.at[src], at.at[src], o_send.at[j], o_recv.at[j],
            device_id={"sp": mate}, device_id_type=MESH,
        ).wait_recv()
        out_desc(j).wait_send()
        return carry

    lax.fori_loop(0, 8, landed, 0)
    for which, out in enumerate((out_n, out_b)):
        values = [at[8 * which + i].astype(F32) for i in range(8)]
        squares = sum(v * v for v in values)
        mean = jnp.sum(squares, axis=-1, keepdims=True) * (1.0 / 1024)
        scale = lax.rsqrt(mean + EPSILON)
        for i in range(8):
            out[0, :, 128 * i : 128 * i + 128] = (values[i] * scale).astype(BF)

    for make in started:
        make().wait_send()


def on_device(ql, kl, rk, qg, kg, nq, bq, nk, nv, bk, bv):
    vmem = pl.BlockSpec(memory_space=pltpu.VMEM)
    hbm = pl.BlockSpec(memory_space=pl.ANY)
    dma = pltpu.SemaphoreType.DMA
    return pl.pallas_call(
        body,
        out_shape=[jax.ShapeDtypeStruct((1, 128, 1024), BF)] * 2,
        in_specs=[vmem] * 9 + [hbm] * 6,
        out_specs=[vmem] * 2,
        scratch_shapes=[
            pltpu.VMEM((24, 768), BF),
            pltpu.VMEM((24, 1280), BF),
            pltpu.VMEM((96, 8, 2048), BF),
            pltpu.VMEM((512, 2560), BF),
            pltpu.VMEM((16, 128, 512), BF),
            pltpu.VMEM((16, 32, 128), BF),
            pltpu.VMEM((2, 128, 768), BF),
            pltpu.VMEM((768, 2048), BF),
            pltpu.VMEM((1024, 512), BF),
            pltpu.VMEM((16, 256, 256), BF),
            pltpu.VMEM((2048, 1536), BF),
            pltpu.VMEM((2048, 128), BF),
            pltpu.VMEM((16, 80, 2048), BF),
            pltpu.VMEM((16, 128, 128), BF),
            pltpu.VMEM((8, 128, 128), BF),
            pltpu.VMEM((256, 128), F32),
            pltpu.VMEM((256, 128), F32),
            pltpu.VMEM((2, 1280, 256), F32),
            pltpu.VMEM((2, 1280, 256), BF),
            pltpu.VMEM((16, 80, 256), F32),
            pltpu.VMEM((2, 16, 1, 256), F32),
            dma((6,)),
            dma((16,)),
            dma((16,)),
            dma((64,)),
            dma((64,)),
            dma((64,)),
            dma((64,)),
            dma((2, 8 * (PZ + 1))),
            dma((2, 8 * (PZ + 1))),
            dma((1,)),
            dma((1,)),
            dma((8,)),
            dma((8,)),
        ],
        compiler_params=pltpu.CompilerParams(
            collective_id=0, has_side_effects=True, vmem_limit_bytes=60 * 1024 * 1024
        ),
        name="latent_attention",
    )(
        ql, kl, jnp.swapaxes(rk, 1, 2), qg.reshape(1, -1), kg.reshape(1, -1),
        *(jnp.asarray(t) for t in rotary_tables()),
        nq, bq, nk, nv, bk, bv,
    )


def solution(mesh):
    in_specs = (
        P("dp", "sp", None),
        P("dp", "sp", None),
        P("dp", "sp", None),
        P(),
        P(),
        P("dp", None),
        P("dp", None),
        P("dp", None),
        P("dp", None),
        P("dp", None),
        P("dp", None),
    )
    out_specs = (P("dp", "sp", None), P("dp", "sp", None))
    return jax.shard_map(
        on_device, mesh=mesh, in_specs=in_specs, out_specs=out_specs, check_vma=False
    )
```

time: 99.3 us -> 73.4 us (0.74)
  the two profiles are of different devices: /device:TPU:32 before, /device:TPU:1 now
where the time goes in v2:
time: 73.4 us; the launch traced here: 73.1 us
  Pallas kernels  68.8 us (94%)
  local copies, waits for them, and re-layouts  3.69 us (5%)
    pallas_call x1, Pallas kernels, on_device(): pl.pallas_call(body, out_shape=[jax.ShapeDtypeStruct((1, 128, 1024), BF)]...  68.8 us
    unnamed x4, local copies, waits for them, and re-layouts  2.42 us

profile of v2, /device:TPU:1, one launch (start us, length us, event | category | flops | bytes accessed | tf_op | source)
XLA Modules:
  0.0 73.1 jit_solution(3004600742338446924)
XLA Ops:
  0.6 1.3 %reshape.10.qg = f32[1,768]{1,0:T(1,128)} reshape(f32[768]{0:T(1024)} %param.18) | data formatting | bytes 6144 | tf_op jit(solution)/shard_map/reshape | solution.py:524
  1.9 68.8 %latent_attention.1 = (bf16[1,128,1024]{2,1,0:T(8,128)(2,1)}, bf16[1,128,1024]{2,1,0:T(8,128)(2,1)}) custom-call(bf16[1,128,768]{2,1,0:T(8,128)(2,1)} %ql.1, bf16[1,128,512]{2,1,0:T(8,128)(2,1)} %kl.1, bf16[1,32,128]{2,1,0:T(8,128)(2,1)} %bitcast.2, f32[1,768]{1,0:T(1,128)} %reshape.10.qg, f32[1,512]{1,0:T(1,128)} %bitcast.3, f32[8,128]{1,0:T(8,128)} %constant.8.clone.ca, ...), custom_call_target="tpu_custom_call" | custom-call | tf_op jit(solution)/shard_map/latent_attention/pallas_call | solution.py:478
  70.7 0.0 copy-start
  70.7 1.7 %copy.19 = bf16[1,128,1024]{2,1,0:T(8,128)(2,1)} copy(bf16[1,128,1024]{2,1,0:T(8,128)(2,1)} %get-tuple-element.4) | data formatting | bytes 524288
  72.4 0.0 copy-done
  72.4 0.7 copy.20
Async XLA Ops:
  70.7 1.7 %copy-start = (bf16[1,128,1024]{2,1,0:T(8,128)(2,1)S(1)}, bf16[1,128,1024]{2,1,0:T(8,128)(2,1)}, u32[]{:S(2)}) copy-start(bf16[1,128,1024]{2,1,0:T(8,128)(2,1)} %get-tuple-element.5) | copy-start | bytes 786436

commit v3 on v2

--- a/solution.py
+++ b/solution.py
@@ -14,6 +14,7 @@
 PZ = 4
 Z_EARLY = 4
 HOOK = 4
+VMEM_LIMIT = 60 * 1024 * 1024
 BF = jnp.bfloat16
 F32 = jnp.float32
 MESH = pl.DeviceIdType.MESH
@@ -43,7 +44,7 @@
 def normalize(latent, gain_row):
     values = latent.astype(F32)
     scaled = values * lax.rsqrt(jnp.mean(values * values, axis=-1, keepdims=True) + EPSILON)
-    return (scaled * gain_row).astype(BF)
+    return (scaled * gain_row[None, :]).astype(BF)
 
 
 def rotate(values, cosine, signed_sine):
@@ -72,6 +73,7 @@
     out_n, out_b,
     raw_n, raw_b, wq8, wkv, kv, rt, qn, wq, wvt, qmt, kp, kr, vt, at, sbuf, cos_t, sin_t,
     s_buf, p_buf, acc_buf, top_buf,
+    v_ql, v_kl, v_rk, v_qg, v_kg, v_ca, v_sa, v_cb, v_sb,
     in_sem, f_send, f_recv, g_send, g_recv, dd_send, dd_recv, z_send, z_recv,
     q_send, q_recv, o_send, o_recv,
 ):
@@ -96,48 +98,53 @@
     def cols(ref, width):
         return ref.at[:, pl.ds(pl.multiple_of(par * width, 128), width)]
 
-    own_rows = pl.ds(pl.multiple_of(d * 16, 16), 16)
-    loads = [
-        pltpu.make_async_copy(cols(nq, 768), raw_n, in_sem.at[0]),
-        pltpu.make_async_copy(cols(bq, 1280), raw_b, in_sem.at[1]),
-        pltpu.make_async_copy(cols(nk, 512), wkv.at[own_rows, pl.ds(0, 512)], in_sem.at[2]),
-        pltpu.make_async_copy(cols(bk, 1024), wkv.at[own_rows, pl.ds(512, 1024)], in_sem.at[3]),
-        pltpu.make_async_copy(cols(nv, 512), wkv.at[own_rows, pl.ds(1536, 512)], in_sem.at[4]),
-        pltpu.make_async_copy(cols(bv, 512), wkv.at[own_rows, pl.ds(2048, 512)], in_sem.at[5]),
-    ]
-    for load in loads:
-        load.start()
-
     barrier = pltpu.get_barrier_semaphore()
     near = [{"sp": zs[1]}, {"sp": zs[-1]}, {"dp": partner_core}]
     near += [{"dp": where[t, k, 0]} for t in range(2) for k in (1, 3)]
     for who in near:
         pl.semaphore_signal(barrier, inc=1, device_id=who, device_id_type=MESH)
 
-    kv[z] = normalize(kl[0], kg[...])
-    half = pl.ds(pl.multiple_of(par * 128, 128), 128)
-    coarse = pl.ds(z // 2, 1)
-    cosine = ca[coarse, :] * cb[...] - sa[coarse, :] * sb[...]
-    sine = sa[coarse, :] * cb[...] + ca[coarse, :] * sb[...]
-    cos_t[...] = cosine
-    sin_t[...] = jnp.where(lane_iota(sine.shape) % 32 < 16, -sine, sine)
-    own_rope = rk[0].astype(F32)
-    rope4 = jnp.concatenate([own_rope] * 4, axis=0).T
-    rope4 = rotate(rope4, cos_t[half, :], sin_t[half, :])
-    rt[z] = rope4.T[:32].astype(BF)
-    qn[par] = normalize(ql[0], qg[...])
+    own_rows = pl.ds(pl.multiple_of(d * 16, 16), 16)
+    pairs = [
+        (cols(nk, 512), wkv.at[own_rows, pl.ds(0, 512)]),
+        (cols(bk, 1024), wkv.at[own_rows, pl.ds(512, 1024)]),
+        (cols(nv, 512), wkv.at[own_rows, pl.ds(1536, 512)]),
+        (cols(bv, 512), wkv.at[own_rows, pl.ds(2048, 512)]),
+        (cols(nq, 768), raw_n),
+        (cols(bq, 1280), raw_b),
+        (kl, v_kl), (kg, v_kg), (rk, v_rk), (ca, v_ca), (sa, v_sa), (cb, v_cb), (sb, v_sb),
+        (ql, v_ql), (qg, v_qg),
+    ]
+    loads = [
+        pltpu.make_async_copy(src, dst, in_sem.at[i]) for i, (src, dst) in enumerate(pairs)
+    ]
     for load in loads:
-        load.wait()
-    wn, wb = raw_n[...].astype(F32), raw_b[...].astype(F32)
-    blocks = [take(wn, [(192 * j, 64), (192 * j + 96, 64)]) for j in range(4)]
-    blocks += [take(wb, [(160 * h, 128)]) for h in range(8)]
-    blocks += [take(wn, [(96 * h + 64, 32) for h in range(4 * g, 4 * g + 4)]) for g in range(2)]
-    blocks += [take(wb, [(160 * h + 128, 32) for h in range(4 * g, 4 * g + 4)]) for g in range(2)]
-    for i, block in enumerate(blocks):
-        for t in range(3):
-            wq8[3 * d + t, :, 128 * i : 128 * i + 128] = block[8 * t : 8 * t + 8].astype(BF)
-
-    pl.semaphore_wait(barrier, 7)
+        load.start()
+
+    def arrange_columns():
+        wn, wb = raw_n[...].astype(F32), raw_b[...].astype(F32)
+        blocks = [take(wn, [(192 * j, 64), (192 * j + 96, 64)]) for j in range(4)]
+        blocks += [take(wb, [(160 * h, 128)]) for h in range(8)]
+        for w, size in ((wn, 96), (wb, 160)):
+            for g in range(0, 8, 4):
+                pieces = [(size * h + size - 32, 32) for h in range(g, g + 4)]
+                blocks.append(take(w, pieces))
+        for i, block in enumerate(blocks):
+            for t in range(3):
+                wq8[3 * d + t, :, 128 * i : 128 * i + 128] = block[8 * t : 8 * t + 8].astype(BF)
+
+    def own_pair():
+        kv[z] = normalize(v_kl[0], v_kg[...])
+        half = pl.ds(pl.multiple_of(par * 128, 128), 128)
+        coarse = pl.ds(z // 2, 1)
+        cosine = v_ca[coarse, :] * v_cb[...] - v_sa[coarse, :] * v_sb[...]
+        sine = v_sa[coarse, :] * v_cb[...] + v_ca[coarse, :] * v_sb[...]
+        cos_t[...] = cosine
+        sin_t[...] = jnp.where(lane_iota(sine.shape) % 32 < 16, -sine, sine)
+        own_rope = v_rk[0].astype(F32)
+        rope4 = jnp.concatenate([own_rope] * 4, axis=0).T
+        rope4 = rotate(rope4, cos_t[half, :], sin_t[half, :])
+        rt[z] = rope4.T[:32].astype(BF)
 
     started = []
 
@@ -229,16 +236,32 @@
         for i in z_pieces(0, 1):
             z_event(step, i)
 
-    for h in range(2):
-        for t in (1, 0):
+    def send_weights(t):
+        for h in range(2):
             for to in (1, -1):
                 start(f_send_copy(t, 0, h, to))
+        for h in range(2):
+            column(t, 0, h)
+
+    for load in loads[:4]:
+        load.wait()
+    pl.semaphore_wait(barrier, 7)
+    send_weights(1)
+    for load in loads[4:6]:
+        load.wait()
+    arrange_columns()
+    for load in loads[6:13]:
+        load.wait()
+    own_pair()
+    send_weights(0)
+    for load in loads[13:]:
+        load.wait()
+    qn[par] = normalize(v_ql[0], v_qg[...])
     for i in z_pieces(0, 1):
         for way in range(2):
             start(z_copy(way, 1, i))
-    for h in range(2):
-        for t in (1, 0):
-            column(t, 0, h)
+    for h in range(16):
+        vt[h, 64:80, :] = jnp.ones((16, 2048), BF)
     mine = qn.at[par]
     start(
         lambda: pltpu.make_async_remote_copy(
@@ -312,9 +335,6 @@
                     head = 4 * (block - 12) + g
                     qmt[head, 128:256, :] = jnp.where(group == g, turned, nothing)
 
-    for h in range(16):
-        vt[h, 64:80, :] = jnp.ones((16, 2048), BF)
-
     def project(b, one, two):
         rows = pl.ds(pl.multiple_of(256 * b, 256), 256)
         x = jnp.concatenate([kv[one], kv[two]], axis=0)
@@ -478,7 +498,7 @@
     return pl.pallas_call(
         body,
         out_shape=[jax.ShapeDtypeStruct((1, 128, 1024), BF)] * 2,
-        in_specs=[vmem] * 9 + [hbm] * 6,
+        in_specs=[hbm] * 15,
         out_specs=[vmem] * 2,
         scratch_shapes=[
             pltpu.VMEM((24, 768), BF),
@@ -502,7 +522,16 @@
             pltpu.VMEM((2, 1280, 256), BF),
             pltpu.VMEM((16, 80, 256), F32),
             pltpu.VMEM((2, 16, 1, 256), F32),
-            dma((6,)),
+            pltpu.VMEM((1, 128, 768), BF),
+            pltpu.VMEM((1, 128, 512), BF),
+            pltpu.VMEM((1, 32, 128), BF),
+            pltpu.VMEM((768,), F32),
+            pltpu.VMEM((512,), F32),
+            pltpu.VMEM((8, 128), F32),
+            pltpu.VMEM((8, 128), F32),
+            pltpu.VMEM((256, 128), F32),
+            pltpu.VMEM((256, 128), F32),
+            dma((15,)),
             dma((16,)),
             dma((16,)),
             dma((64,)),
@@ -517,11 +546,11 @@
             dma((8,)),
         ],
         compiler_params=pltpu.CompilerParams(
-            collective_id=0, has_side_effects=True, vmem_limit_bytes=60 * 1024 * 1024
+            collective_id=0, has_side_effects=True, vmem_limit_bytes=VMEM_LIMIT
         ),
         name="latent_attention",
     )(
-        ql, kl, jnp.swapaxes(rk, 1, 2), qg.reshape(1, -1), kg.reshape(1, -1),
+        ql, kl, jnp.swapaxes(rk, 1, 2), qg, kg,
         *(jnp.asarray(t) for t in rotary_tables()),
         nq, bq, nk, nv, bk, bv,
     )

time: 73.4 us -> 71.4 us (0.973)
  local copies, waits for them, and re-layouts: 3.69 us -> 2.42 us
    reshape x1 -> x0, local copies, waits for them, and re-layouts: 1.27 us -> none  [on_device(): qg.reshape(1, -1)]
where the time goes in v3:
time: 71.4 us; the launch traced here: 71.3 us
  Pallas kernels  68.2 us (96%)
  local copies, waits for them, and re-layouts  2.42 us (3%)
    pallas_call x1, Pallas kernels, on_device(): pl.pallas_call(body, out_shape=[jax.ShapeDtypeStruct((1, 128, 1024), BF)]...  68.2 us
    unnamed x4, local copies, waits for them, and re-layouts  2.42 us

profile of v3, /device:TPU:1, one launch (start us, length us, event | category | flops | bytes accessed | tf_op | source)
XLA Modules:
  0.0 71.3 jit_solution(4475452107607182885)
XLA Ops:
  0.6 68.2 %latent_attention.1 = (bf16[1,128,1024]{2,1,0:T(8,128)(2,1)}, bf16[1,128,1024]{2,1,0:T(8,128)(2,1)}) custom-call(bf16[1,128,768]{2,1,0:T(8,128)(2,1)} %ql.1, bf16[1,128,512]{2,1,0:T(8,128)(2,1)} %kl.1, bf16[1,32,128]{2,1,0:T(8,128)(2,1)} %bitcast.1, f32[768]{0:T(1024)} %qg.1, f32[512]{0:T(512)} %kg.1, f32[8,128]{1,0:T(8,128)} %constant.8.clone.ca, ...), custom_call_target="tpu_custom_call" | custom-call | tf_op jit(solution)/shard_map/latent_attention/pallas_call | solution.py:498
  68.9 0.0 copy-start
  68.9 1.7 %copy.19 = bf16[1,128,1024]{2,1,0:T(8,128)(2,1)} copy(bf16[1,128,1024]{2,1,0:T(8,128)(2,1)} %get-tuple-element.4) | data formatting | bytes 524288
  70.6 0.0 copy-done
  70.6 0.7 copy.20
Async XLA Ops:
  68.9 1.7 %copy-start = (bf16[1,128,1024]{2,1,0:T(8,128)(2,1)S(1)}, bf16[1,128,1024]{2,1,0:T(8,128)(2,1)}, u32[]{:S(2)}) copy-start(bf16[1,128,1024]{2,1,0:T(8,128)(2,1)} %get-tuple-element.5) | copy-start | bytes 786436

commit v4 on v3

--- a/solution.py
+++ b/solution.py
@@ -299,6 +299,9 @@
                         ref, ref, dd_send.at[index], dd_recv.at[index],
                         device_id={"dp": partner_core}, device_id_type=MESH,
                     ).wait_recv()
+        if t == 1:
+            for i in range(8):
+                wvt[128 * i : 128 * i + 128, :] = wkv[:, 1536 + 128 * i : 1664 + 128 * i].T
     theirs = qn.at[1 - par]
     pltpu.make_async_remote_copy(
         theirs, theirs, q_send.at[0], q_recv.at[0], device_id={"sp": mate}, device_id_type=MESH
@@ -310,8 +313,6 @@
         return carry
 
     lax.fori_loop(0, 48, pack_rows, 0)
-    for i in range(8):
-        wvt[128 * i : 128 * i + 128, :] = wkv[:, 1536 + 128 * i : 1664 + 128 * i].T
 
     tokens = jnp.concatenate([qn[0], qn[1]], axis=0)
     group = row_iota((128, 256)) // 32
@@ -427,8 +428,9 @@
             soften(0, b, first_top, factor_of(0))
         second_top = all_scores(1, 1)
 
-        def step(i, top):
-            hook(i)
+        def step(i, top, tail=False):
+            if not tail:
+                hook(i)
             parts = []
             for k in range(2):
                 h = 2 * i + k
@@ -437,21 +439,24 @@
                 sums = gather(h, k)
                 peak = None
                 for b in range(count):
-                    found = score(ahead, k, b)
-                    peak = found if peak is None else jnp.maximum(peak, found)
-                    soften(1 - k, b, top, factor)
+                    if not tail:
+                        found = score(ahead, k, b)
+                        peak = found if peak is None else jnp.maximum(peak, found)
+                    if not tail or k == 0:
+                        soften(1 - k, b, top, factor)
                 if last:
                     kept = jnp.exp2((top_buf[0, h] - top_buf[1, h]) * factor_of(h))
                     whole = acc_buf[h] * kept + sums
                     parts.append(whole[0:64] / whole[64:65])
                 else:
                     acc_buf[h] = sums
-                top = settle(ahead, peak)
+                if not tail:
+                    top = settle(ahead, peak)
             if last:
                 finish_pair(i, parts)
             return top
 
-        lax.fori_loop(0, 8, step, second_top)
+        step(7, lax.fori_loop(0, 7, step, second_top), tail=True)
 
     for step in range(Z_EARLY + 1, 6):
         z_step(step)

time: 71.4 us -> 71 us (level)
  no operation moved by 1% of the time
where the time goes in v4:
time: 71 us; the launch traced here: 70.9 us
  Pallas kernels  67.8 us (95%)
  local copies, waits for them, and re-layouts  2.42 us (3%)
    pallas_call x1, Pallas kernels, on_device(): pl.pallas_call(body, out_shape=[jax.ShapeDtypeStruct((1, 128, 1024), BF)]...  67.8 us
    unnamed x4, local copies, waits for them, and re-layouts  2.42 us

profile of v4, /device:TPU:1, one launch (start us, length us, event | category | flops | bytes accessed | tf_op | source)
XLA Modules:
  0.0 70.9 jit_solution(1214923597339890120)
XLA Ops:
  0.6 67.8 %latent_attention.1 = (bf16[1,128,1024]{2,1,0:T(8,128)(2,1)}, bf16[1,128,1024]{2,1,0:T(8,128)(2,1)}) custom-call(bf16[1,128,768]{2,1,0:T(8,128)(2,1)} %ql.1, bf16[1,128,512]{2,1,0:T(8,128)(2,1)} %kl.1, bf16[1,32,128]{2,1,0:T(8,128)(2,1)} %bitcast.1, f32[768]{0:T(1024)} %qg.1, f32[512]{0:T(512)} %kg.1, f32[8,128]{1,0:T(8,128)} %constant.8.clone.ca, ...), custom_call_target="tpu_custom_call" | custom-call | tf_op jit(solution)/shard_map/latent_attention/pallas_call | solution.py:503
  68.4 0.0 copy-start
  68.4 1.7 %copy.19 = bf16[1,128,1024]{2,1,0:T(8,128)(2,1)} copy(bf16[1,128,1024]{2,1,0:T(8,128)(2,1)} %get-tuple-element.4) | data formatting | bytes 524288
  70.2 0.0 copy-done
  70.2 0.7 copy.20
Async XLA Ops:
  68.4 1.7 %copy-start = (bf16[1,128,1024]{2,1,0:T(8,128)(2,1)S(1)}, bf16[1,128,1024]{2,1,0:T(8,128)(2,1)}, u32[]{:S(2)}) copy-start(bf16[1,128,1024]{2,1,0:T(8,128)(2,1)} %get-tuple-element.5) | copy-start | bytes 786436
